TPU v7x, 768 devices: a whole 4x8x12 slice. The times are simulated.
768 devices in a mesh: ep: 48 (over z, x), tp: 16 (over y, core).
Axes of the slice: x: 4, y: 8, z: 12, core: 2. Of those that a mesh axis runs over, the one named last changes fastest.
Arguments:
- tokens: bfloat16 [768, 2048], P('ep'), may hold values from -6 to 6
- attn_gain: bfloat16 [2048], replicated, may hold values from 0.099609375 to 1.8984375
- ffn_gain: bfloat16 [2048], replicated, may hold values from 0.099609375 to 1.8984375
- w_query: bfloat16 [2048, 2048], P(None, 'tp'), may hold values from -0.125 to 0.125
- w_key: bfloat16 [2048, 256], replicated, may hold values from -0.125 to 0.125
- w_value: bfloat16 [2048, 256], replicated, may hold values from -0.125 to 0.125
- w_forget: bfloat16 [2048, 32], replicated, may hold values from -0.125 to 0.125
- forget_bias: float32 [32], replicated, may hold values from -1 to 3
- w_out: bfloat16 [2048, 2048], P(None, 'tp'), may hold values from -0.375 to 0.375
- cache_keys: bfloat16 [768, 2048, 256], P(('ep', 'tp')), may hold values from -800 to 800
- cache_values: bfloat16 [768, 2048, 256], P(('ep', 'tp')), may hold values from -6 to 6
- cache_logcum: float32 [768, 32, 2048], P(('ep', 'tp')), as said below
- cache_len: int32 [768], P(('ep', 'tp')), may hold values from 256 to 2048
- route_group: int32 [768], P('ep'), may hold values from 0 to 3, as said below
- route_expert: int32 [768, 2], P('ep'), may hold values from 0 to 11, as said below
- route_weight: float32 [768, 2], P('ep'), may hold values from 0.2 to 1
- w_gate: bfloat16 [48, 2048, 2048], P('ep', None, 'tp'), may hold values from -0.125 to 0.125
- w_up: bfloat16 [48, 2048, 2048], P('ep', None, 'tp'), may hold values from -0.125 to 0.125
- w_down: bfloat16 [48, 2048, 2048], P('ep', None, 'tp'), may hold values from -0.125 to 0.125
Outputs:
- layer_out: bfloat16 [768, 2048], P('ep', 'tp')
Inputs may be any that keep to these rules, and one draw needn't show every extreme that they name: Expert groups. Among the 16 sequences of one index of ep no expert route_group * 12 + route_expert is named more than 2 times, and in every draw one expert is named exactly 2 times by the sequences of every index of ep. `route_expert`: the 2 numbers of a sequence differ. `cache_logcum`: each entry is the sum of the log forget gates of that head from the first cached position up to and including that position.
All inputs are finite; a program needn't handle non-finite values.
Results may differ from a plain program's by a relative error of at most 0.012.
The roundings to bfloat16 on the way count: a program that leaves them out, or rounds other values in their place, can miss the bound.
Values may be sent and summed in bfloat16 or wider, within the bound.
A program may use at most 32 MiB of HBM per device.

v0:
```python
import jax
import jax.numpy as jnp
from jax import lax
from jax.sharding import PartitionSpec as P

QUERY_HEAD_COUNT = 32
KV_HEADS = 4
HEAD = 64
GROUPS = 4
TOP = 2


NORM_EPSILON = 1e-06
MASKED_SCORE = -1e30


def copy_for_each(value, axis):
    length = lax.axis_size(axis)
    return lax.all_to_all(
        jnp.broadcast_to(value[None], (length, *value.shape)), axis, 0, 0, tiled=True
    )


def laid_out(pieces, dim):
    shape = list(pieces.shape[1:])
    shape[dim] *= pieces.shape[0]
    return jnp.moveaxis(pieces, 0, dim).reshape(shape)


def collect(value, axis, dim):
    pieces = copy_for_each(value, axis)
    return laid_out(pieces, dim)


def normalize(values, gain_vec):
    return (
        values
        * lax.rsqrt(jnp.mean(values * values, axis=-1, keepdims=True) + NORM_EPSILON)
        * gain_vec.astype(jnp.float32)
    )


def attend(query, key_new, value_new, log_gate, keys, cached_values, logcum, lengths):
    count_of_rows = query.shape[0]
    length = keys.shape[1]
    per_kv = QUERY_HEAD_COUNT // KV_HEADS
    score_scale = HEAD ** (-0.5)
    query_half = query.reshape(count_of_rows, KV_HEADS, per_kv, HEAD)
    keys_h = keys.reshape(count_of_rows, length, KV_HEADS, HEAD)
    scores = jnp.einsum("bkgd,blkd->bkgl", query_half, keys_h, preferred_element_type=jnp.float32)
    scores = scores.reshape(count_of_rows, QUERY_HEAD_COUNT, length) * score_scale
    latest = jnp.take_along_axis(logcum, (lengths - 1)[:, None, None], axis=2)
    scores = scores + latest + log_gate[:, :, None] - logcum
    usable = jnp.arange(length, dtype=jnp.int32)[None, None, :] < lengths[:, None, None]
    scores = jnp.where(usable, scores, MASKED_SCORE)
    current_key = key_new.reshape(count_of_rows, KV_HEADS, HEAD)
    current_score = jnp.einsum(
        "cnpx,cnx->cnp", query_half, current_key, preferred_element_type=jnp.float32
    )
    current_score = current_score.reshape(count_of_rows, QUERY_HEAD_COUNT) * score_scale
    peak = jnp.maximum(jnp.max(scores, axis=2), current_score)
    weights = jnp.where(usable, jnp.exp(scores - peak[:, :, None]), 0.0)
    own_weight = jnp.exp(current_score - peak)
    denominator = jnp.sum(weights, axis=2) + own_weight
    weights_b = weights.astype(jnp.bfloat16).reshape(count_of_rows, KV_HEADS, per_kv, length)
    own_b = (
        own_weight.astype(jnp.bfloat16).astype(jnp.float32).reshape(count_of_rows, KV_HEADS, per_kv)
    )
    values_h = cached_values.reshape(count_of_rows, length, KV_HEADS, HEAD)
    summed = jnp.einsum("bkgl,blkd->bkgd", weights_b, values_h, preferred_element_type=jnp.float32)
    own_value = value_new.astype(jnp.float32).reshape(count_of_rows, KV_HEADS, 1, HEAD)
    summed = summed + own_b[..., None] * own_value
    summed = summed.reshape(count_of_rows, QUERY_HEAD_COUNT, HEAD) / denominator[:, :, None]
    return summed.reshape(count_of_rows, QUERY_HEAD_COUNT * HEAD).astype(jnp.bfloat16)


def on_device(
    tokens,
    attn_gain,
    ffn_gain,
    w_query,
    w_key,
    w_value,
    w_forget,
    forget_bias,
    w_out,
    cache_keys,
    cache_values,
    cache_logcum,
    cache_len,
    route_group,
    route_expert,
    route_weight,
    w_gate,
    w_up,
    w_down,
):
    tp_index = lax.axis_index("tp")
    expert_count = lax.axis_size("ep")
    group_rows = tokens.shape[0]
    own_rows = cache_len.shape[0]
    width_part = w_out.shape[1]
    stream = tokens.astype(jnp.float32)
    normed = normalize(stream, attn_gain).astype(jnp.bfloat16)
    query_part = jnp.dot(normed, w_query, preferred_element_type=jnp.float32).astype(jnp.bfloat16)
    query = lax.all_to_all(query_part, "tp", split_axis=0, concat_axis=1, tiled=True)
    own_normed = lax.dynamic_slice_in_dim(normed, tp_index * own_rows, own_rows, 0)
    key_new = jnp.dot(own_normed, w_key, preferred_element_type=jnp.float32).astype(jnp.bfloat16)
    value_new = jnp.dot(own_normed, w_value, preferred_element_type=jnp.float32).astype(
        jnp.bfloat16
    )
    log_gate = jax.nn.log_sigmoid(
        jnp.dot(own_normed, w_forget, preferred_element_type=jnp.float32) + forget_bias
    )
    attended = attend(
        query, key_new, value_new, log_gate, cache_keys, cache_values, cache_logcum, cache_len
    )
    projected = jnp.dot(collect(attended, "tp", 0), w_out, preferred_element_type=jnp.float32)
    residual = lax.dynamic_slice_in_dim(stream, tp_index * width_part, width_part, 1)
    mixed = (residual + projected).astype(jnp.bfloat16)
    per_group = expert_count // GROUPS
    capacity = max(2, (group_rows + per_group // 2 - 1) // per_group + 1)
    picked_ids = (route_group[:, None] * per_group + route_expert).reshape(-1)
    chosen = (picked_ids[:, None] == jnp.arange(expert_count, dtype=jnp.int32)[None, :]).astype(
        jnp.int32
    )
    earlier = jnp.cumsum(chosen, axis=0) - chosen
    slot_index = jnp.sum(earlier * chosen, axis=1)
    target = picked_ids * capacity + slot_index
    place_table = (
        target[:, None] == jnp.arange(expert_count * capacity, dtype=jnp.int32)[None, :]
    ).astype(jnp.float32)
    place_table = place_table.reshape(group_rows, TOP, expert_count * capacity)
    send_table = jnp.sum(place_table, axis=1).astype(jnp.bfloat16)
    combine = jnp.sum(route_weight[:, :, None] * place_table, axis=1)
    packed = jnp.einsum("sp,sd->pd", send_table, mixed, preferred_element_type=jnp.float32).astype(
        jnp.bfloat16
    )
    full_rows = lax.all_gather(
        lax.all_to_all(
            packed.reshape(expert_count, capacity, mixed.shape[1]),
            "ep",
            split_axis=0,
            concat_axis=0,
            tiled=True,
        ),
        "tp",
        axis=2,
        tiled=True,
    )
    sources, slot_count, row_width = full_rows.shape
    flat_rows = full_rows.reshape(sources * slot_count, row_width)
    inputs = normalize(flat_rows.astype(jnp.float32), ffn_gain).astype(jnp.bfloat16)
    gate_proj = jnp.dot(inputs, w_gate[0], preferred_element_type=jnp.float32)
    up_proj = jnp.dot(inputs, w_up[0], preferred_element_type=jnp.float32)
    hidden = (jax.nn.silu(gate_proj) * up_proj).astype(jnp.bfloat16)
    rows_down = w_down[0]
    summed = jnp.dot(
        lax.all_gather(hidden, "tp", axis=1, tiled=True),
        rows_down,
        preferred_element_type=jnp.float32,
    )
    returned = summed.astype(jnp.bfloat16).reshape(sources, slot_count, w_down.shape[2])
    returned_rows = lax.all_to_all(returned, "ep", split_axis=0, concat_axis=0, tiled=True)
    moe_sum = jnp.dot(
        combine,
        returned_rows.reshape(-1, width_part).astype(jnp.float32),
        precision=lax.Precision.HIGHEST,
    )
    return (mixed.astype(jnp.float32) + moe_sum).astype(jnp.bfloat16)


def solution(mesh):
    placed = (
        P("ep", None),
        P(),
        P(),
        P(None, "tp"),
        P(),
        P(),
        P(),
        P(),
        P(None, "tp"),
        P(("ep", "tp"), None, None),
        P(("ep", "tp"), None, None),
        P(("ep", "tp"), None, None),
        P(("ep", "tp")),
        P("ep"),
        P("ep", None),
        P("ep", None),
        P("ep", None, "tp"),
        P("ep", None, "tp"),
        P("ep", None, "tp"),
    )
    return jax.shard_map(
        on_device, mesh=mesh, in_specs=placed, out_specs=P("ep", "tp"), check_vma=False
    )
```

profile of v0, /device:TPU:1, one launch (start us, length us, event | category | flops | bytes accessed | tf_op | source)
XLA Modules:
  0.0 123.1 jit_solution(4986807858427267003)
XLA Ops:
  0.0 0.8 convert_element_type.94
  0.9 1.0 multiply_reduce_fusion
  1.9 1.2 fusion.8
  3.1 0.6 copy.49
  3.8 13.8 %all-to-all-start = ((bf16[16,1,128]{2,1,0:T(2,128)(2,1)}), bf16[16,1,128]{2,1,0:T(2,128)(2,1)S(1)}, u32[]{:S(2)}, u32[]{:S(2)}) async-start(bf16[16,1,128]{2,1,0:T(2,128)(2,1)} %copy.49), calls=%async_computation | async-start | bytes 16384 | tf_op jit(solution)/shard_map/all_to_all | solution.py:106
  18.7 0.7 copy-done.10
  21.2 1.5 %copy.50 = bf16[1,2048,256]{1,2,0:T(8,128)(2,1)S(1)} copy(bf16[1,2048,256]{2,1,0:T(8,128)(2,1)} %param.28) | data formatting | bytes 2097152 | tf_op args[9]
  22.8 1.5 %copy.51 = bf16[1,2048,256]{1,2,0:T(8,128)(2,1)S(1)} copy(bf16[1,2048,256]{2,1,0:T(8,128)(2,1)} %param.29) | data formatting | bytes 2097152 | tf_op args[10]
  24.4 0.9 select_reduce_fusion
  25.5 1.3 %fusion.41 = (f32[32]{0:T(128)S(1)}, f32[1,32,2048]{2,1,0:T(8,128)S(1)}) fusion(f32[1,32,2048]{2,1,0:T(8,128)} %param.30, f32[32]{0:T(128)S(1)} %fusion.37, f32[32]{0:T(128)S(1)} %select_reduce_fusion, bf16[4,8,64]{2,1,0:T(8,128)(2,1)S(1)} %reshape.324, bf16[2048,4,64]{0,2,1:T(8,128)(2,1)S(1)} %bitcast.77, pred[2048]{0:T(1024)(128)(4,1)S(1)} %iota_compare_fusion.2), kind=kOutput, calls=%fused_computation.72 | convolution fusion | flops 8781792 | bytes 1579392 | tf_op jit(solution)/shard_map/bkgd,blkd->bkgl/dot_general | solution.py:50
  28.7 1.0 reduce.10
  29.7 0.7 reshape.397
  30.3 7.3 %all-to-all-start.1 = ((bf16[16,2,1024]{2,1,0:T(2,128)(2,1)}), bf16[16,2,1024]{2,1,0:T(2,128)(2,1)S(1)}, u32[]{:S(2)}, u32[]{:S(2)}) async-start(bf16[16,2,1024]{2,1,0:T(2,128)(2,1)} %reshape.397), calls=%async_computation.1 | async-start | bytes 131072 | tf_op jit(solution)/shard_map/all_to_all | solution.py:19
  37.8 0.7 copy-done.9
  38.5 6.8 %all-to-all-done.1 = bf16[16,2,1024]{2,1,0:T(2,128)(2,1)S(1)} async-done(((bf16[16,2,1024]{2,1,0:T(2,128)(2,1)}), bf16[16,2,1024]{2,1,0:T(2,128)(2,1)S(1)}, u32[]{:S(2)}, u32[]{:S(2)}) %all-to-all-start.1) | async-done | bytes 65568 | tf_op jit(solution)/shard_map/all_to_all | solution.py:19
  45.6 0.8 convolution_convert_fusion.1
  46.4 13.0 %all-to-all-start.2 = ((bf16[48,2,128]{2,1,0:T(2,128)(2,1)}), bf16[48,2,128]{2,1,0:T(2,128)(2,1)S(1)}, u32[]{:S(2)}, u32[]{:S(2)}) async-start(bf16[48,2,128]{2,1,0:T(2,128)(2,1)} %bitcast.14), calls=%async_computation.2 | async-start | bytes 49152 | tf_op jit(solution)/shard_map/all_to_all | solution.py:140
  59.4 10.9 %all-to-all-done.2 = bf16[48,2,128]{2,1,0:T(2,128)(2,1)S(1)} async-done(((bf16[48,2,128]{2,1,0:T(2,128)(2,1)}), bf16[48,2,128]{2,1,0:T(2,128)(2,1)S(1)}, u32[]{:S(2)}, u32[]{:S(2)}) %all-to-all-start.2) | async-done | bytes 24608 | tf_op jit(solution)/shard_map/all_to_all | solution.py:140
  70.2 17.2 %all_gather.6 = bf16[48,2,2048]{2,1,0:T(2,128)(2,1)S(1)} all-gather(bf16[48,2,128]{2,1,0:T(2,128)(2,1)S(1)} %all-to-all-done.2), channel_id=1, replica_groups=mesh['ep'=48,'tp'=16] {'tp'}, dimensions={2}, use_global_device_ids=true | all-gather | bytes 417792 | tf_op jit(solution)/shard_map/all_gather | solution.py:139
  88.6 0.9 copy-done.5
  89.8 0.8 copy-done.6
  90.8 16.5 %all_gather.7 = bf16[96,2048]{1,0:T(8,128)(2,1)S(1)} all-gather(bf16[96,128]{1,0:T(8,128)(2,1)S(1)} %fusion.5), channel_id=1, replica_groups=mesh['ep'=48,'tp'=16] {'tp'}, dimensions={1}, use_global_device_ids=true | all-gather | bytes 417792 | tf_op jit(solution)/shard_map/all_gather | solution.py:159
  107.6 14.7 %all_to_all.28 = bf16[48,2,128]{2,1,0:T(2,128)(2,1)S(1)} all-to-all(bf16[48,2,128]{2,1,0:T(2,128)(2,1)S(1)} %bitcast.79), channel_id=1, replica_groups=mesh['ep'=48,'tp'=16] {'ep'}, dimensions={0} | all-to-all | bytes 49152 | tf_op jit(solution)/shard_map/all_to_all | solution.py:164
  122.3 0.7 fusion.6
  (71 shorter events, 7.0 us)
Async XLA Ops:
  0.0 18.2 %copy-start = (bf16[2048,256]{1,0:T(8,128)(2,1)S(1)}, bf16[2048,256]{1,0:T(8,128)(2,1)}, u32[]{:S(2)}) copy-start(bf16[2048,256]{1,0:T(8,128)(2,1)} %param.23) | copy-start | bytes 3145732
  0.0 1.8 %copy-start.2 = (bf16[16,2048]{1,0:T(8,128)(2,1)S(1)}, bf16[16,2048]{1,0:T(8,128)(2,1)}, u32[]{:S(2)}) copy-start(bf16[16,2048]{1,0:T(8,128)(2,1)} %param.19) | copy-start | bytes 196612
  0.0 18.4 %copy-start.1 = (bf16[2048,256]{1,0:T(8,128)(2,1)S(1)}, bf16[2048,256]{1,0:T(8,128)(2,1)}, u32[]{:S(2)}) copy-start(bf16[2048,256]{1,0:T(8,128)(2,1)} %param.24) | copy-start | bytes 3145732
  3.8 21.6 %all-to-all-start = ((bf16[16,1,128]{2,1,0:T(2,128)(2,1)}), bf16[16,1,128]{2,1,0:T(2,128)(2,1)S(1)}, u32[]{:S(2)}, u32[]{:S(2)}) async-start(bf16[16,1,128]{2,1,0:T(2,128)(2,1)} %copy.49), calls=%async_computation | async-start | bytes 16384 | tf_op jit(solution)/shard_map/all_to_all | solution.py:106
  18.4 2.1 %copy-start.7 = (bf16[2048,32]{0,1:T(8,128)(2,1)S(1)}, bf16[2048,32]{0,1:T(8,128)(2,1)}, u32[]{:S(2)}) copy-start(bf16[2048,32]{0,1:T(8,128)(2,1)} %param.25) | copy-start | bytes 393220
  18.7 0.7 copy-start.10
  19.4 0.7 copy-start.12
  20.3 0.7 copy-start.11
  28.0 17.4 %copy-start.4 = (bf16[2048,128]{1,0:T(8,128)(2,1)S(1)}, bf16[2048,128]{1,0:T(8,128)(2,1)}, u32[]{:S(2)}) copy-start(bf16[2048,128]{1,0:T(8,128)(2,1)} %param.27) | copy-start | bytes 1572868
  30.3 15.0 %all-to-all-start.1 = ((bf16[16,2,1024]{2,1,0:T(2,128)(2,1)}), bf16[16,2,1024]{2,1,0:T(2,128)(2,1)S(1)}, u32[]{:S(2)}, u32[]{:S(2)}) async-start(bf16[16,2,1024]{2,1,0:T(2,128)(2,1)} %reshape.397), calls=%async_computation.1 | async-start | bytes 131072 | tf_op jit(solution)/shard_map/all_to_all | solution.py:19
  37.8 0.7 copy-start.9
  46.4 13.0 %copy-start.8 = (bf16[2048]{0:T(1024)(128)(2,1)S(1)}, bf16[2048]{0:T(1024)(128)(2,1)}, u32[]{:S(2)}) copy-start(bf16[2048]{0:T(1024)(128)(2,1)} %param.21) | copy-start | bytes 12292
  46.4 23.8 %all-to-all-start.2 = ((bf16[48,2,128]{2,1,0:T(2,128)(2,1)}), bf16[48,2,128]{2,1,0:T(2,128)(2,1)S(1)}, u32[]{:S(2)}, u32[]{:S(2)}) async-start(bf16[48,2,128]{2,1,0:T(2,128)(2,1)} %bitcast.14), calls=%async_computation.2 | async-start | bytes 49152 | tf_op jit(solution)/shard_map/all_to_all | solution.py:140
  88.5 1.0 copy-start.5
  89.5 1.0 copy-start.6
  90.6 16.8 %copy-start.3 = (bf16[1,2048,128]{2,1,0:T(8,128)(2,1)S(1)}, bf16[1,2048,128]{2,1,0:T(8,128)(2,1)}, u32[]{:S(2)}) copy-start(bf16[1,2048,128]{2,1,0:T(8,128)(2,1)} %param.37) | copy-start | bytes 1572868
where the time goes:
time: 124 us; the launch traced here: 123 us
  blocking collectives  48.5 us (39%)
  starting transfers between devices  34 us (27%)
  waiting for transfers between devices  17.7 us (14%)
  local copies, waits for them, and re-layouts  10.1 us (8%)
  matrix products  6.23 us (5%)
  other arithmetic  5.65 us (5%)
    all_gather x1, blocking collectives, on_device(): lax.all_gather(lax.all_to_all(packed.reshape(expert_count, capacity, mixe...  17.2 us
    all_gather x1, blocking collectives, on_device(): lax.all_gather(hidden, 'tp', axis=1, tiled=True)  16.5 us
    all_to_all x1, blocking collectives, on_device(): lax.all_to_all(returned, 'ep', split_axis=0, concat_axis=0, tiled=True)  14.7 us
    all_to_all x1, starting transfers between devices, on_device(): lax.all_to_all(query_part, 'tp', split_axis=0, concat_axis=1, tiled=True)  13.8 us
    all_to_all x1, starting transfers between devices, on_device(): lax.all_to_all(packed.reshape(expert_count, capacity, mixed.shape[1]), 'e...  13 us
    all_to_all x1, waiting for transfers between devices, on_device(): lax.all_to_all(packed.reshape(expert_count, capacity, mixed.shape[1]), 'e...  10.9 us
    unnamed x31, local copies, waits for them, and re-layouts  7.85 us
    all_to_all x1, starting transfers between devices, copy_for_each(): lax.all_to_all(jnp.broadcast_to(value[None], (length, *value.shape)), axi...  7.27 us
  transfers between devices with their start and end apart: 3, of which 2 were waited for; matrix products, arithmetic and copies ran while one was open for 5% of the time, Pallas kernels for 0%

commit v1 on v0

v1 whole, which is shorter than its diff:
```python
import functools

import jax
import jax.numpy as jnp
from jax import lax
from jax.experimental import pallas as pl
from jax.experimental.pallas import tpu as pltpu
from jax.sharding import PartitionSpec as P

HEADS = 32
KV_HEADS = 4
HEAD = 64
GROUPS = 4
EPSILON = 1e-06
MASKED_SCORE = -1e30
SLOTS = 2
BF = jnp.bfloat16
F32 = jnp.float32
MESH = pl.DeviceIdType.MESH


def iota(shape, dim):
    return lax.broadcasted_iota(jnp.int32, shape, dim)


def dot(a, b):
    return jnp.dot(a, b, preferred_element_type=F32)


def dot_t(a, b):
    return lax.dot_general(a, b, (((1,), (1,)), ((), ())), preferred_element_type=F32)


def exact_parts(x):
    a = x.astype(BF)
    r = x - a.astype(F32)
    b = r.astype(BF)
    return a, b, (r - b.astype(F32)).astype(BF)


def layer_kernel(n_ep, n_tp, *refs):
    inputs, out_ref, rest = refs[:19], refs[19], refs[20:]
    held, scratch = rest[:18], rest[18:]
    (tok, again, fgain, wq, wk, wv, wf, fb, wo, ck, cv, lc, rg, re, rw, wg, wu, wd) = held
    len_ref = scratch[-1]
    sources = inputs[:12] + inputs[13:]
    (
        q_send, q_recv, att_all, att_rows, d_send, d_recv, x_all, h_all, r_send, r_recv,
        in_sem, q_ss, q_rs, a_ss, a_rs, d_ss, d_rs, x_ss, x_rs, x_fs, x_ps, h_ss, h_rs, h_fs, h_ps,
        r_ss, r_rs, len_sem, _,
    ) = scratch
    e = lax.axis_index("ep")
    t = lax.axis_index("tp")
    n_y = n_tp // 2
    y, c = t // 2, t % 2
    rows = tok.shape[0]
    picks = n_ep * SLOTS
    width = wo.shape[1]

    def ep_peer(i):
        k = (i + 1) // 2
        return lax.rem(e + n_ep // 2 + k * (1 - 2 * (i % 2)) + n_ep, n_ep)

    def tp_peer(i):
        k = (i + 1) // 2
        return lax.rem(t + n_tp // 2 + k * (1 - 2 * (i % 2)) + n_tp, n_tp)

    def loads(i):
        return pltpu.make_async_copy(sources[i], held[i], in_sem.at[i])

    for i in (0, 1, 3, 4, 5, 6, 7, 9, 11, 10, 12, 13, 14, 8, 2, 15, 16, 17):
        loads(i).start()
    load_len = pltpu.make_async_copy(inputs[12], len_ref, len_sem)
    load_len.start()

    barrier = pltpu.get_barrier_semaphore()

    @pl.loop(0, n_tp - 1)
    def _(i):
        pl.semaphore_signal(barrier, inc=1, device_id=(e, tp_peer(i)), device_id_type=MESH)

    @pl.loop(0, n_ep - 1)
    def _(i):
        pl.semaphore_signal(barrier, inc=1, device_id=(ep_peer(i), t), device_id_type=MESH)

    loads(0).wait()
    loads(1).wait()
    stream = tok[...].astype(F32)
    scale = lax.rsqrt(jnp.mean(stream * stream, axis=-1, keepdims=True) + EPSILON)
    normed = (stream * scale * again[...].reshape(1, -1).astype(F32)).astype(BF)
    loads(3).wait()
    q_send[...] = dot(normed, wq[...]).astype(BF).astype(F32)
    pl.semaphore_wait(barrier, n_tp - 1 + n_ep - 1)

    def q_copy(i):
        to = tp_peer(i)
        return pltpu.make_async_remote_copy(
            src_ref=q_send.at[pl.ds(to, 1)], dst_ref=q_recv.at[pl.ds(t, 1)],
            send_sem=q_ss, recv_sem=q_rs, device_id=(e, to), device_id_type=MESH,
        )

    @pl.loop(0, n_tp - 1)
    def _(i):
        q_copy(i).start()

    own = iota((rows, 1), 0) == t
    for i in (4, 5, 6, 7):
        loads(i).wait()

    def own_row(value):
        return jnp.sum(jnp.where(own, value, 0.0), axis=0, keepdims=True)

    key_new = own_row(dot(normed, wk[...])).astype(BF).astype(F32)
    value_new = own_row(dot(normed, wv[...])).astype(BF).astype(F32)
    eye = iota((HEADS, HEADS), 0) == iota((HEADS, HEADS), 1)
    bias = jnp.sum(jnp.where(eye, fb[...].reshape(1, -1), 0.0), axis=1, keepdims=True)
    gate_all = dot_t(wf[...], normed)
    own_lane = iota((1, rows), 1) == t
    gate_in = jnp.sum(jnp.where(own_lane, gate_all, 0.0), axis=1, keepdims=True) + bias
    log_gate = jnp.minimum(gate_in, 0.0) - jnp.log1p(jnp.exp(-jnp.abs(gate_in)))
    loads(11).wait()
    load_len.wait()
    length = len_ref[0]
    logcum = lc[0]
    position = iota((1, logcum.shape[1]), 1)
    latest = jnp.sum(jnp.where(position == length - 1, logcum, 0.0), axis=1, keepdims=True)

    for i in (12, 13, 14):
        loads(i).wait()
    eye_rows = iota((rows, rows), 0) == iota((rows, rows), 1)

    def column(row, zero):
        return jnp.sum(jnp.where(eye_rows, row, zero), axis=1, keepdims=True)

    chosen = rg[...].reshape(1, -1) * (n_ep // GROUPS) + re[...]
    slot_row = iota((picks, rows), 0)
    named = jnp.logical_or(
        chosen[0:1, :] == slot_row // SLOTS, chosen[1:2, :] == slot_row // SLOTS
    )
    named = named.astype(F32)
    before = (iota((rows, rows), 0) < iota((rows, rows), 1)).astype(F32).astype(BF)
    earlier = dot(named.astype(BF), before)
    place = jnp.where(earlier == (slot_row % SLOTS).astype(F32), named, 0.0).astype(BF)
    slot_lane = iota((rows, picks), 1)
    first = column(chosen[0:1, :], 0) == slot_lane // SLOTS
    second = column(chosen[1:2, :], 0) == slot_lane // SLOTS
    named_t = jnp.logical_or(first, second).astype(F32)
    before_t = (iota((rows, rows), 1) < iota((rows, rows), 0)).astype(F32).astype(BF)
    earlier_t = dot(before_t, named_t.astype(BF))
    here = earlier_t == (slot_lane % SLOTS).astype(F32)
    weight_t = jnp.where(first, column(rw[0:1, :], 0.0), column(rw[1:2, :], 0.0))
    combine = exact_parts(jnp.where(here, named_t * weight_t, 0.0))

    pltpu.make_async_copy(q_recv.at[pl.ds(0, n_tp - 1)], q_recv.at[pl.ds(0, n_tp - 1)], q_rs).wait()
    q16 = jnp.where(iota((n_tp, 1), 0) == t, q_send[...], q_recv[...])
    twice = (iota((HEADS, n_tp), 0) // 2 == iota((HEADS, n_tp), 1)).astype(F32).astype(BF)
    q32 = dot(twice, q16.astype(BF))
    turned = pltpu.roll(q32, HEAD, 1)
    odd = iota((HEADS, 2 * HEAD), 0) % 2 == 1
    low = iota((HEADS, 2 * HEAD), 1) < HEAD
    q_both = jnp.where(odd == low, turned, q32)
    q_wide = jnp.concatenate([q_both] * (KV_HEADS // 2), axis=1)
    kv_width = KV_HEADS * HEAD
    mine = iota((HEADS, kv_width), 1) // HEAD == iota((HEADS, kv_width), 0) // (HEADS // KV_HEADS)
    q_wide = jnp.where(mine, q_wide, 0.0)
    score_scale = HEAD ** (-0.5)
    own_score = jnp.sum(q_wide * key_new, axis=1, keepdims=True) * score_scale
    loads(9).wait()
    scores = dot_t(q_wide.astype(BF), ck[0]) * score_scale
    scores = scores + latest + log_gate - logcum
    usable = position < length
    scores = jnp.where(usable, scores, MASKED_SCORE)
    peak = jnp.maximum(jnp.max(scores, axis=1, keepdims=True), own_score)
    weights = jnp.where(usable, jnp.exp(scores - peak), 0.0)
    own_weight = jnp.exp(own_score - peak)
    denominator = jnp.sum(weights, axis=1, keepdims=True) + own_weight
    loads(10).wait()
    summed = dot(weights.astype(BF), cv[0])
    summed = summed + own_weight.astype(BF).astype(F32) * value_new
    summed = jnp.where(mine, summed, 0.0)
    folded = summed[:, : 2 * HEAD]
    for k in range(1, KV_HEADS // 2):
        folded = folded + summed[:, k * 2 * HEAD : (k + 1) * 2 * HEAD]
    folded = ((folded + pltpu.roll(folded, HEAD, 1)) / denominator).astype(BF)
    pair = iota((n_tp, HEADS), 1) - 2 * iota((n_tp, HEADS), 0)
    even_rows = dot((pair == 0).astype(F32).astype(BF), folded)
    odd_rows = dot((pair == 1).astype(F32).astype(BF), folded)
    att_all[t] = jnp.where(iota((n_tp, 2 * HEAD), 1) < HEAD, even_rows, odd_rows).astype(BF)

    def att_copy(i):
        return pltpu.make_async_remote_copy(
            src_ref=att_all.at[t], dst_ref=att_all.at[t],
            send_sem=a_ss, recv_sem=a_rs, device_id=(e, tp_peer(i)), device_id_type=MESH,
        )

    @pl.loop(0, n_tp - 1)
    def _(i):
        att_copy(i).start()

    residual = tok[:, pl.ds(pl.multiple_of(t * width, width), width)].astype(F32)
    loads(8).wait()
    pltpu.make_async_copy(
        att_all.at[pl.ds(0, n_tp - 1)], att_all.at[pl.ds(0, n_tp - 1)], a_rs
    ).wait()
    att_rows[...] = att_all[...].reshape(n_tp * n_tp, 2 * HEAD).astype(F32)
    attended = jnp.concatenate(
        [att_rows[pl.ds(k, n_tp, stride=n_tp), :].astype(BF) for k in range(n_tp)], axis=1
    )
    mixed = (residual + dot(attended, wo[...])).astype(BF)

    d_send[...] = dot(place, mixed).astype(BF)

    def pick_copy(i, src, dst, ss, rs):
        to = ep_peer(i)
        return pltpu.make_async_remote_copy(
            src_ref=src.at[pl.ds(pl.multiple_of(to * SLOTS, SLOTS), SLOTS)],
            dst_ref=dst.at[pl.ds(pl.multiple_of(e * SLOTS, SLOTS), SLOTS)],
            send_sem=ss, recv_sem=rs, device_id=(to, t), device_id_type=MESH,
        )

    def all_picks(ref, sem):
        part = ref.at[pl.ds(0, picks - SLOTS)]
        return pltpu.make_async_copy(part, part, sem)

    @pl.loop(0, n_ep - 1)
    def _(i):
        pick_copy(i, d_send, d_recv, d_ss, d_rs).start()

    own_slots = iota((picks, 1), 0) // SLOTS == e
    all_picks(d_recv, d_rs).wait()
    x_all[t] = jnp.where(own_slots, d_send[...].astype(F32), d_recv[...].astype(F32)).astype(BF)

    far_first = sorted(range(1, n_y), key=lambda d: -min(d, n_y - d))
    partner = 2 * y + 1 - c

    def column_copy(buf, d, ss, rs):
        to = 2 * lax.rem(y + d, n_y) + c
        return pltpu.make_async_remote_copy(
            src_ref=buf.at[t], dst_ref=buf.at[t],
            send_sem=ss.at[d], recv_sem=rs.at[d], device_id=(e, to), device_id_type=MESH,
        )

    def pass_on(buf, d, fs, ps):
        slot = 2 * lax.rem(y + n_y - d, n_y) + c
        return pltpu.make_async_remote_copy(
            src_ref=buf.at[slot], dst_ref=buf.at[slot],
            send_sem=fs.at[d], recv_sem=ps.at[d], device_id=(e, partner), device_id_type=MESH,
        )

    def gather(buf, ss, rs, fs, ps):
        for d in far_first:
            column_copy(buf, d, ss, rs).start()
        pass_on(buf, 0, fs, ps).start()
        for d in far_first[::-1]:
            column_copy(buf, d, ss, rs).wait_recv()
            pass_on(buf, d, fs, ps).start()
        for d in range(n_y):
            pass_on(buf, d, fs, ps).wait_recv()

    def gather_end(buf, ss, rs, fs, ps):
        for d in range(n_y):
            if d:
                column_copy(buf, d, ss, rs).wait_send()
            pass_on(buf, d, fs, ps).wait_send()

    gather(x_all, x_ss, x_rs, x_fs, x_ps)
    for i in (2, 15, 16, 17):
        loads(i).wait()
    total = jnp.zeros((picks, width), F32)
    for k in range(n_tp):
        part = x_all[k].astype(F32)
        total = total + part * part
    scale = lax.rsqrt(jnp.sum(total, axis=1, keepdims=True) / (n_tp * width) + EPSILON)
    gain = fgain[...].reshape(1, -1).astype(F32)
    moe_in = jnp.concatenate(
        [
            (x_all[k].astype(F32) * scale * gain[:, k * width : (k + 1) * width]).astype(BF)
            for k in range(n_tp)
        ],
        axis=1,
    )
    gated = dot(moe_in, wg[0])
    up = dot(moe_in, wu[0])
    h_all[t] = (gated / (1.0 + jnp.exp(-gated)) * up).astype(BF)
    gather(h_all, h_ss, h_rs, h_fs, h_ps)
    hidden = jnp.concatenate([h_all[k] for k in range(n_tp)], axis=1)
    r_send[...] = dot(hidden, wd[0]).astype(BF)

    @pl.loop(0, n_ep - 1)
    def _(i):
        pick_copy(i, r_send, r_recv, r_ss, r_rs).start()

    all_picks(r_recv, r_rs).wait()
    back = jnp.where(own_slots, r_send[...].astype(F32), r_recv[...].astype(F32)).astype(BF)
    moe_sum = sum(dot(part, back) for part in combine[::-1])
    out_ref[...] = (mixed.astype(F32) + moe_sum).astype(BF)

    pltpu.make_async_copy(q_send.at[pl.ds(0, n_tp - 1)], q_send.at[pl.ds(0, n_tp - 1)], q_ss).wait()
    pltpu.make_async_copy(
        att_all.at[pl.ds(0, n_tp - 1)], att_all.at[pl.ds(0, n_tp - 1)], a_ss
    ).wait()
    all_picks(d_send, d_ss).wait()
    gather_end(x_all, x_ss, x_rs, x_fs, x_ps)
    gather_end(h_all, h_ss, h_rs, h_fs, h_ps)
    all_picks(r_send, r_ss).wait()


def on_device(*args):
    args = list(args)
    for i in (6, 14, 15):
        args[i] = args[i].T
    n_ep = lax.axis_size("ep")
    n_tp = lax.axis_size("tp")
    rows = args[0].shape[0]
    width = args[8].shape[1]
    picks = n_ep * SLOTS
    any_spec = pl.BlockSpec(memory_space=pl.ANY)
    specs = [any_spec] * 19
    held = [pltpu.VMEM(a.shape, a.dtype) for i, a in enumerate(args) if i != 12]
    dma = pltpu.SemaphoreType.DMA
    n_y = n_tp // 2
    scratch = held + [
        pltpu.VMEM((rows, width), F32),
        pltpu.VMEM((n_tp, width), F32),
        pltpu.VMEM((n_tp, n_tp, 2 * HEAD), BF),
        pltpu.VMEM((n_tp * n_tp, 2 * HEAD), F32),
        pltpu.VMEM((picks, width), BF),
        pltpu.VMEM((picks, width), BF),
        pltpu.VMEM((n_tp, picks, width), BF),
        pltpu.VMEM((n_tp, picks, width), BF),
        pltpu.VMEM((picks, width), BF),
        pltpu.VMEM((picks, width), BF),
        dma((18,)),
        dma, dma, dma, dma, dma, dma,
        dma((n_y,)), dma((n_y,)), dma((n_y,)), dma((n_y,)),
        dma((n_y,)), dma((n_y,)), dma((n_y,)), dma((n_y,)),
        dma, dma, dma, pltpu.SMEM((1,), jnp.int32),
    ]
    return pl.pallas_call(
        functools.partial(layer_kernel, n_ep, n_tp),
        out_shape=jax.ShapeDtypeStruct((rows, width), BF),
        in_specs=specs,
        out_specs=pl.BlockSpec(memory_space=pltpu.VMEM),
        scratch_shapes=scratch,
        compiler_params=pltpu.CompilerParams(
            collective_id=0, has_side_effects=True, vmem_limit_bytes=60 * 1024 * 1024
        ),
        name="layer",
    )(*args)


def solution(mesh):
    placed = (
        P("ep", None),
        P(),
        P(),
        P(None, "tp"),
        P(),
        P(),
        P(),
        P(),
        P(None, "tp"),
        P(("ep", "tp"), None, None),
        P(("ep", "tp"), None, None),
        P(("ep", "tp"), None, None),
        P(("ep", "tp")),
        P("ep"),
        P("ep", None),
        P("ep", None),
        P("ep", None, "tp"),
        P("ep", None, "tp"),
        P("ep", None, "tp"),
    )
    return jax.shard_map(
        on_device, mesh=mesh, in_specs=placed, out_specs=P("ep", "tp"), check_vma=False
    )
```

time: 124 us -> 64.3 us (0.52)
  Pallas kernels: 0 us -> 62.2 us
  blocking collectives: 48.5 us -> 0 us
  starting transfers between devices: 34 us -> 0 us
  waiting for transfers between devices: 17.7 us -> 0 us
  local copies, waits for them, and re-layouts: 10.1 us -> 1.28 us
  matrix products: 6.23 us -> 0 us
  other arithmetic: 5.65 us -> 0 us
    pallas_call x0 -> x1, Pallas kernels: none -> 62.2 us  [on_device(): pl.pallas_call(functools.partial(layer_kernel, n_ep, n_tp), out_shape=jax...]
    all_to_all x3 -> x0, starting transfers between devices: 34 us -> none  [the longest x1 13.8 us: on_device(): lax.all_to_all(query_part, 'tp', split_axis=0, concat_axis=1, tiled=True)]
    all_gather x2 -> x0, blocking collectives: 33.8 us -> none  [the longest x1 17.2 us: on_device(): lax.all_gather(lax.all_to_all(packed.reshape(expert_count, capacity, mixe...]
    all_to_all x3 -> x0, waiting for transfers between devices: 17.7 us -> none  [the longest x1 10.9 us: on_device(): lax.all_to_all(packed.reshape(expert_count, capacity, mixed.shape[1]), 'e...]
    all_to_all x1 -> x0, blocking collectives: 14.7 us -> none  [on_device(): lax.all_to_all(returned, 'ep', split_axis=0, concat_axis=0, tiled=True)]
    unnamed x31 -> x1, local copies, waits for them, and re-layouts: 7.85 us -> 1.28 us
    dot_general x13 -> x0, matrix products: 6.23 us -> none  [the longest x1 1.31 us: attend(): jnp.einsum('bkgd,blkd->bkgl', query_half, keys_h, preferred_element_type=...]
    reduce_sum x5 -> x0, other arithmetic: 1.95 us -> none  [the longest x2 1.45 us: normalize(): jnp.mean(values * values, axis=-1, keepdims=True) + NORM_EPSILON]
  transfers between devices with their start and end apart: 3 -> 0, of which waited for: 2 -> 0; matrix products, arithmetic and copies ran while one was open for 5% -> 0% of each run, Pallas kernels for 0% -> 0%
where the time goes in v1:
time: 64.3 us; the launch traced here: 64.2 us
  Pallas kernels  62.2 us (97%)
  local copies, waits for them, and re-layouts  1.28 us (2%)
  between operations  0.66 us (1%)
    pallas_call x1, Pallas kernels, on_device(): pl.pallas_call(functools.partial(layer_kernel, n_ep, n_tp), out_shape=jax...  62.2 us

profile of v1, /device:TPU:1, one launch (start us, length us, event | category | flops | bytes accessed | tf_op | source)
XLA Modules:
  0.0 64.2 jit_solution(2881056980587873086)
XLA Ops:
  0.7 62.2 %layer.1 = bf16[16,128]{1,0:T(8,128)(2,1)} custom-call(bf16[16,2048]{1,0:T(8,128)(2,1)} %refs_0_.1, bf16[2048]{0:T(1024)(128)(2,1)} %refs_1_.1, bf16[2048]{0:T(1024)(128)(2,1)} %refs_2_.1, bf16[2048,128]{1,0:T(8,128)(2,1)} %refs_3_.1, bf16[2048,256]{1,0:T(8,128)(2,1)} %refs_4_.1, bf16[2048,256]{1,0:T(8,128)(2,1)} %refs_5_.1, bf16[32,2048]{1,0:T(8,128)(2,1)} %bitcast.3, ...), custom_call_target="tpu_custom_call" | custom-call | tf_op jit(solution)/shard_map/layer/pallas_call | solution.py:339
  62.9 1.3 %copy.22 = bf16[16,128]{1,0:T(8,128)(2,1)} copy(bf16[16,128]{1,0:T(8,128)(2,1)} %layer.1) | data formatting | bytes 8192

commit v2 on v1

--- a/solution.py
+++ b/solution.py
@@ -38,17 +38,23 @@
     return a, b, (r - b.astype(F32)).astype(BF)
 
 
-def layer_kernel(n_ep, n_tp, *refs):
+def layer_kernel(n_ep, n_tp, bounds, *refs):
     inputs, out_ref, rest = refs[:19], refs[19], refs[20:]
     held, scratch = rest[:18], rest[18:]
     (tok, again, fgain, wq, wk, wv, wf, fb, wo, ck, cv, lc, rg, re, rw, wg, wu, wd) = held
-    len_ref = scratch[-1]
     sources = inputs[:12] + inputs[13:]
-    (
-        q_send, q_recv, att_all, att_rows, d_send, d_recv, x_all, h_all, r_send, r_recv,
-        in_sem, q_ss, q_rs, a_ss, a_rs, d_ss, d_rs, x_ss, x_rs, x_fs, x_ps, h_ss, h_rs, h_fs, h_ps,
-        r_ss, r_rs, len_sem, _,
-    ) = scratch
+    count = len(bounds) - 1
+    scratch = list(scratch)
+
+    def take(number):
+        taken = scratch[:number]
+        del scratch[:number]
+        return taken
+
+    q_send, q_recv, att_all, att_rows, d_send, d_recv, r_send, r_recv, len_ref = take(9)
+    x_all, h_all = take(count), take(count)
+    in_sem, len_sem, q_ss, q_rs, a_ss, a_rs, d_ss, d_rs, r_ss, r_rs, ready = take(11)
+    x_sems, h_sems = take(count), take(count)
     e = lax.axis_index("ep")
     t = lax.axis_index("tp")
     n_y = n_tp // 2
@@ -68,10 +74,9 @@
     def loads(i):
         return pltpu.make_async_copy(sources[i], held[i], in_sem.at[i])
 
-    for i in (0, 1, 3, 4, 5, 6, 7, 9, 11, 10, 12, 13, 14, 8, 2, 15, 16, 17):
+    for i in (0, 1, 3):
         loads(i).start()
     load_len = pltpu.make_async_copy(inputs[12], len_ref, len_sem)
-    load_len.start()
 
     barrier = pltpu.get_barrier_semaphore()
 
@@ -79,9 +84,9 @@
     def _(i):
         pl.semaphore_signal(barrier, inc=1, device_id=(e, tp_peer(i)), device_id_type=MESH)
 
-    @pl.loop(0, n_ep - 1)
-    def _(i):
-        pl.semaphore_signal(barrier, inc=1, device_id=(ep_peer(i), t), device_id_type=MESH)
+    @pl.loop(0, n_ep - 1 - e)
+    def _(i):
+        pl.semaphore_signal(barrier, inc=1, device_id=(n_ep - 1 - i, t), device_id_type=MESH)
 
     loads(0).wait()
     loads(1).wait()
@@ -89,8 +94,13 @@
     scale = lax.rsqrt(jnp.mean(stream * stream, axis=-1, keepdims=True) + EPSILON)
     normed = (stream * scale * again[...].reshape(1, -1).astype(F32)).astype(BF)
     loads(3).wait()
+    for i in (4, 5, 6, 7, 11):
+        loads(i).start()
+    load_len.start()
+    for i in (12, 13, 14, 9, 10, 8, 2, 15, 16, 17):
+        loads(i).start()
     q_send[...] = dot(normed, wq[...]).astype(BF).astype(F32)
-    pl.semaphore_wait(barrier, n_tp - 1 + n_ep - 1)
+    pl.semaphore_wait(barrier, n_tp - 1 + e)
 
     def q_copy(i):
         to = tp_peer(i)
@@ -99,9 +109,13 @@
             send_sem=q_ss, recv_sem=q_rs, device_id=(e, to), device_id_type=MESH,
         )
 
-    @pl.loop(0, n_tp - 1)
+    @pl.loop(0, n_tp - 1, unroll=True)
     def _(i):
         q_copy(i).start()
+
+    @pl.loop(0, e)
+    def _(i):
+        pl.semaphore_signal(ready, inc=1, device_id=(i, t), device_id_type=MESH)
 
     own = iota((rows, 1), 0) == t
     for i in (4, 5, 6, 7):
@@ -193,7 +207,7 @@
             send_sem=a_ss, recv_sem=a_rs, device_id=(e, tp_peer(i)), device_id_type=MESH,
         )
 
-    @pl.loop(0, n_tp - 1)
+    @pl.loop(0, n_tp - 1, unroll=True)
     def _(i):
         att_copy(i).start()
 
@@ -210,99 +224,151 @@
 
     d_send[...] = dot(place, mixed).astype(BF)
 
-    def pick_copy(i, src, dst, ss, rs):
-        to = ep_peer(i)
+    @pl.when(e < n_ep - 1)
+    def _():
+        pl.semaphore_wait(ready, n_ep - 1 - e)
+
+    def pick_copy(to, src, dst, ss, rs):
         return pltpu.make_async_remote_copy(
             src_ref=src.at[pl.ds(pl.multiple_of(to * SLOTS, SLOTS), SLOTS)],
             dst_ref=dst.at[pl.ds(pl.multiple_of(e * SLOTS, SLOTS), SLOTS)],
             send_sem=ss, recv_sem=rs, device_id=(to, t), device_id_type=MESH,
         )
 
-    def all_picks(ref, sem):
-        part = ref.at[pl.ds(0, picks - SLOTS)]
-        return pltpu.make_async_copy(part, part, sem)
-
-    @pl.loop(0, n_ep - 1)
-    def _(i):
-        pick_copy(i, d_send, d_recv, d_ss, d_rs).start()
+    def slots_wait(ref, sem, count):
+        part = ref.at[pl.ds(0, count * SLOTS)]
+        return pltpu.make_async_copy(part, part, sem).wait()
+
+    batch = sum((e >= first).astype(jnp.int32) for first in bounds[1:-1])
+
+    @pl.loop(0, n_ep - 1, unroll=True)
+    def _(i):
+        pick_copy(ep_peer(i), d_send, d_recv, d_ss, d_rs.at[batch]).start()
 
     own_slots = iota((picks, 1), 0) // SLOTS == e
-    all_picks(d_recv, d_rs).wait()
-    x_all[t] = jnp.where(own_slots, d_send[...].astype(F32), d_recv[...].astype(F32)).astype(BF)
-
     far_first = sorted(range(1, n_y), key=lambda d: -min(d, n_y - d))
     partner = 2 * y + 1 - c
 
-    def column_copy(buf, d, ss, rs):
+    def column_copy(buf, d, sems):
         to = 2 * lax.rem(y + d, n_y) + c
         return pltpu.make_async_remote_copy(
             src_ref=buf.at[t], dst_ref=buf.at[t],
-            send_sem=ss.at[d], recv_sem=rs.at[d], device_id=(e, to), device_id_type=MESH,
-        )
-
-    def pass_on(buf, d, fs, ps):
+            send_sem=sems.at[0, d], recv_sem=sems.at[1, d], device_id=(e, to), device_id_type=MESH,
+        )
+
+    def pass_on(buf, d, sems):
         slot = 2 * lax.rem(y + n_y - d, n_y) + c
         return pltpu.make_async_remote_copy(
             src_ref=buf.at[slot], dst_ref=buf.at[slot],
-            send_sem=fs.at[d], recv_sem=ps.at[d], device_id=(e, partner), device_id_type=MESH,
-        )
-
-    def gather(buf, ss, rs, fs, ps):
+            send_sem=sems.at[2, d], recv_sem=sems.at[3, d], device_id=(e, partner), device_id_type=MESH,
+        )
+
+    def gather_start(buf, sems):
         for d in far_first:
-            column_copy(buf, d, ss, rs).start()
-        pass_on(buf, 0, fs, ps).start()
+            column_copy(buf, d, sems).start()
+        pass_on(buf, 0, sems).start()
+
+    def gather_pass(buf, sems):
         for d in far_first[::-1]:
-            column_copy(buf, d, ss, rs).wait_recv()
-            pass_on(buf, d, fs, ps).start()
+            column_copy(buf, d, sems).wait_recv()
+            pass_on(buf, d, sems).start()
+
+    def gather_finish(buf, sems):
         for d in range(n_y):
-            pass_on(buf, d, fs, ps).wait_recv()
-
-    def gather_end(buf, ss, rs, fs, ps):
+            pass_on(buf, d, sems).wait_recv()
+
+    def gather_end(buf, sems):
         for d in range(n_y):
             if d:
-                column_copy(buf, d, ss, rs).wait_send()
-            pass_on(buf, d, fs, ps).wait_send()
-
-    gather(x_all, x_ss, x_rs, x_fs, x_ps)
-    for i in (2, 15, 16, 17):
-        loads(i).wait()
-    total = jnp.zeros((picks, width), F32)
-    for k in range(n_tp):
-        part = x_all[k].astype(F32)
-        total = total + part * part
-    scale = lax.rsqrt(jnp.sum(total, axis=1, keepdims=True) / (n_tp * width) + EPSILON)
-    gain = fgain[...].reshape(1, -1).astype(F32)
-    moe_in = jnp.concatenate(
-        [
-            (x_all[k].astype(F32) * scale * gain[:, k * width : (k + 1) * width]).astype(BF)
-            for k in range(n_tp)
-        ],
-        axis=1,
-    )
-    gated = dot(moe_in, wg[0])
-    up = dot(moe_in, wu[0])
-    h_all[t] = (gated / (1.0 + jnp.exp(-gated)) * up).astype(BF)
-    gather(h_all, h_ss, h_rs, h_fs, h_ps)
-    hidden = jnp.concatenate([h_all[k] for k in range(n_tp)], axis=1)
-    r_send[...] = dot(hidden, wd[0]).astype(BF)
-
-    @pl.loop(0, n_ep - 1)
-    def _(i):
-        pick_copy(i, r_send, r_recv, r_ss, r_rs).start()
-
-    all_picks(r_recv, r_rs).wait()
+                column_copy(buf, d, sems).wait_send()
+            pass_on(buf, d, sems).wait_send()
+
+    def arrive(k):
+        count = bounds[k + 1] - bounds[k]
+        slots = slice(bounds[k] * SLOTS, bounds[k + 1] * SLOTS)
+
+        @pl.when(batch == k)
+        def _():
+            slots_wait(d_recv, d_rs.at[k], count - 1)
+
+        @pl.when(batch != k)
+        def _():
+            slots_wait(d_recv, d_rs.at[k], count)
+
+        x_all[k][t] = jnp.where(
+            own_slots[slots], d_send[slots, :].astype(F32), d_recv[slots, :].astype(F32)
+        ).astype(BF)
+        gather_start(x_all[k], x_sems[k])
+
+    def expand(k):
+        gather_finish(x_all[k], x_sems[k])
+        if k == 0:
+            for i in (2, 15, 16, 17):
+                loads(i).wait()
+        buf = x_all[k]
+        total = jnp.zeros(buf.shape[1:], F32)
+        for j in range(n_tp):
+            part = buf[j].astype(F32)
+            total = total + part * part
+        scale = lax.rsqrt(jnp.sum(total, axis=1, keepdims=True) / (n_tp * width) + EPSILON)
+        gain = fgain[...].reshape(1, -1).astype(F32)
+        moe_in = jnp.concatenate(
+            [
+                (buf[j].astype(F32) * scale * gain[:, j * width : (j + 1) * width]).astype(BF)
+                for j in range(n_tp)
+            ],
+            axis=1,
+        )
+        gated = dot(moe_in, wg[0])
+        up = dot(moe_in, wu[0])
+        h_all[k][t] = (gated / (1.0 + jnp.exp(-gated)) * up).astype(BF)
+        gather_start(h_all[k], h_sems[k])
+
+    def contract(k):
+        slots = slice(bounds[k] * SLOTS, bounds[k + 1] * SLOTS)
+        gather_finish(h_all[k], h_sems[k])
+        hidden = jnp.concatenate([h_all[k][j] for j in range(n_tp)], axis=1)
+        r_send[slots, :] = dot(hidden, wd[0]).astype(BF)
+
+        @pl.loop(0, n_ep - 1, unroll=True)
+        def _(i):
+            to = ep_peer(i)
+
+            @pl.when(jnp.logical_and(to >= bounds[k], to < bounds[k + 1]))
+            def _():
+                pick_copy(to, r_send, r_recv, r_ss, r_rs).start()
+
+    n_batches = len(bounds) - 1
+    arrive(0)
+    gather_pass(x_all[0], x_sems[0])
+    expand(0)
+    for k in range(1, n_batches):
+        arrive(k)
+        gather_pass(h_all[k - 1], h_sems[k - 1])
+        gather_pass(x_all[k], x_sems[k])
+        contract(k - 1)
+        expand(k)
+    gather_pass(h_all[n_batches - 1], h_sems[n_batches - 1])
+    contract(n_batches - 1)
+
+    slots_wait(r_recv, r_rs, n_ep - 1)
     back = jnp.where(own_slots, r_send[...].astype(F32), r_recv[...].astype(F32)).astype(BF)
     moe_sum = sum(dot(part, back) for part in combine[::-1])
-    out_ref[...] = (mixed.astype(F32) + moe_sum).astype(BF)
+    out_ref[...] = mixed.astype(F32) + moe_sum
 
     pltpu.make_async_copy(q_send.at[pl.ds(0, n_tp - 1)], q_send.at[pl.ds(0, n_tp - 1)], q_ss).wait()
     pltpu.make_async_copy(
         att_all.at[pl.ds(0, n_tp - 1)], att_all.at[pl.ds(0, n_tp - 1)], a_ss
     ).wait()
-    all_picks(d_send, d_ss).wait()
-    gather_end(x_all, x_ss, x_rs, x_fs, x_ps)
-    gather_end(h_all, h_ss, h_rs, h_fs, h_ps)
-    all_picks(r_send, r_ss).wait()
+    slots_wait(d_send, d_ss, n_ep - 1)
+    for k in range(n_batches):
+        gather_end(x_all[k], x_sems[k])
+        gather_end(h_all[k], h_sems[k])
+    slots_wait(r_send, r_ss, n_ep - 1)
+
+
+def batch_bounds(n_ep):
+    return (0, n_ep // 3, n_ep)
 
 
 def on_device(*args):
@@ -314,11 +380,12 @@
     rows = args[0].shape[0]
     width = args[8].shape[1]
     picks = n_ep * SLOTS
-    any_spec = pl.BlockSpec(memory_space=pl.ANY)
+    bounds = batch_bounds(n_ep)
+    sizes = [(b - a) * SLOTS for a, b in zip(bounds, bounds[1:])]
+    any_spec = pl.BlockSpec(memory_space=pltpu.HBM)
     specs = [any_spec] * 19
     held = [pltpu.VMEM(a.shape, a.dtype) for i, a in enumerate(args) if i != 12]
     dma = pltpu.SemaphoreType.DMA
-    n_y = n_tp // 2
     scratch = held + [
         pltpu.VMEM((rows, width), F32),
         pltpu.VMEM((n_tp, width), F32),
@@ -326,27 +393,29 @@
         pltpu.VMEM((n_tp * n_tp, 2 * HEAD), F32),
         pltpu.VMEM((picks, width), BF),
         pltpu.VMEM((picks, width), BF),
-        pltpu.VMEM((n_tp, picks, width), BF),
-        pltpu.VMEM((n_tp, picks, width), BF),
         pltpu.VMEM((picks, width), BF),
         pltpu.VMEM((picks, width), BF),
-        dma((18,)),
-        dma, dma, dma, dma, dma, dma,
-        dma((n_y,)), dma((n_y,)), dma((n_y,)), dma((n_y,)),
-        dma((n_y,)), dma((n_y,)), dma((n_y,)), dma((n_y,)),
-        dma, dma, dma, pltpu.SMEM((1,), jnp.int32),
+        pltpu.SMEM((1,), jnp.int32),
+    ]
+    scratch += [pltpu.VMEM((n_tp, size, width), BF) for size in sizes + sizes]
+    scratch += [dma((18,)), dma, dma, dma, dma, dma, dma, dma((len(sizes),)), dma, dma]
+    scratch += [pltpu.SemaphoreType.REGULAR]
+    scratch += [dma((4, n_tp // 2)) for _ in sizes + sizes]
+    args = [
+        a if i == 12 else pltpu.with_memory_space_constraint(a, pltpu.HBM)
+        for i, a in enumerate(args)
     ]
     return pl.pallas_call(
-        functools.partial(layer_kernel, n_ep, n_tp),
-        out_shape=jax.ShapeDtypeStruct((rows, width), BF),
+        functools.partial(layer_kernel, n_ep, n_tp, bounds),
+        out_shape=jax.ShapeDtypeStruct((rows, width), F32),
         in_specs=specs,
         out_specs=pl.BlockSpec(memory_space=pltpu.VMEM),
         scratch_shapes=scratch,
         compiler_params=pltpu.CompilerParams(
-            collective_id=0, has_side_effects=True, vmem_limit_bytes=60 * 1024 * 1024
+            collective_id=0, has_side_effects=True, vmem_limit_bytes=24 * 1024 * 1024
         ),
         name="layer",
-    )(*args)
+    )(*args).astype(BF)
 
 
 def solution(mesh):

time: 64.3 us -> 54.9 us (0.85)
  Pallas kernels: 62.2 us -> 53.5 us
  local copies, waits for them, and re-layouts: 1.28 us -> 0 us
    pallas_call x1, Pallas kernels: 62.2 us -> 53.5 us  [on_device(): pl.pallas_call(functools.partial(layer_kernel, n_ep, n_tp, bounds), out_s...]
    unnamed x1 -> x0, local copies, waits for them, and re-layouts: 1.28 us -> none
where the time goes in v2:
time: 54.9 us; the launch traced here: 54.7 us
  Pallas kernels  53.5 us (97%)
  between operations  0.66 us (1%)
  other arithmetic  0.6 us (1%)
    pallas_call x1, Pallas kernels, on_device(): pl.pallas_call(functools.partial(layer_kernel, n_ep, n_tp, bounds), out_s...  53.5 us

profile of v2, /device:TPU:1, one launch (start us, length us, event | category | flops | bytes accessed | tf_op | source)
XLA Modules:
  0.0 54.7 jit_solution(8277875311351468849)
XLA Ops:
  0.7 53.5 %layer.1 = f32[16,128]{1,0:T(8,128)S(1)} custom-call(bf16[16,2048]{1,0:T(8,128)(2,1)} %refs_0_.1, bf16[2048]{0:T(1024)(128)(2,1)} %refs_1_.1, bf16[2048]{0:T(1024)(128)(2,1)} %refs_2_.1, bf16[2048,128]{1,0:T(8,128)(2,1)} %refs_3_.1, bf16[2048,256]{1,0:T(8,128)(2,1)} %refs_4_.1, bf16[2048,256]{1,0:T(8,128)(2,1)} %refs_5_.1, bf16[32,2048]{1,0:T(8,128)(2,1)} %bitcast.3, ...), custom_call_target="tpu_custom_call" | custom-call | tf_op jit(solution)/shard_map/layer/pallas_call | solution.py:408
  54.1 0.6 %convert_element_type.3 = bf16[16,128]{1,0:T(8,128)(2,1)} convert(f32[16,128]{1,0:T(8,128)S(1)} %layer.1) | non-fusion elementwise | flops 2048 | bytes 12288 | tf_op jit(solution)/shard_map/convert_element_type | solution.py:418

commit v3 on v2

--- a/solution.py
+++ b/solution.py
@@ -38,7 +38,7 @@
     return a, b, (r - b.astype(F32)).astype(BF)
 
 
-def layer_kernel(n_ep, n_tp, bounds, *refs):
+def layer_kernel(n_ep, n_tp, bounds, orders, *refs):
     inputs, out_ref, rest = refs[:19], refs[19], refs[20:]
     held, scratch = rest[:18], rest[18:]
     (tok, again, fgain, wq, wk, wv, wf, fb, wo, ck, cv, lc, rg, re, rw, wg, wu, wd) = held
@@ -54,18 +54,25 @@
     q_send, q_recv, att_all, att_rows, d_send, d_recv, r_send, r_recv, len_ref = take(9)
     x_all, h_all = take(count), take(count)
     in_sem, len_sem, q_ss, q_rs, a_ss, a_rs, d_ss, d_rs, r_ss, r_rs, ready = take(11)
-    x_sems, h_sems = take(count), take(count)
-    e = lax.axis_index("ep")
+    x_sems = list(zip(take(count), take(count)))
+    h_sems = list(zip(take(count), take(count)))
+    ep = lax.axis_index("ep")
+    zero_rank = n_ep // 3 - 1
+
+    def rank_of(place):
+        return jnp.where(place == 0, zero_rank, place - (place <= zero_rank).astype(jnp.int32))
+
+    e = rank_of(ep)
     t = lax.axis_index("tp")
     n_y = n_tp // 2
     y, c = t // 2, t % 2
     rows = tok.shape[0]
+    late = n_ep * 2 // 3
     picks = n_ep * SLOTS
     width = wo.shape[1]
 
-    def ep_peer(i):
-        k = (i + 1) // 2
-        return lax.rem(e + n_ep // 2 + k * (1 - 2 * (i % 2)) + n_ep, n_ep)
+    def at_rank(rank):
+        return jnp.where(rank == zero_rank, 0, rank + (rank < zero_rank).astype(jnp.int32))
 
     def tp_peer(i):
         k = (i + 1) // 2
@@ -82,11 +89,11 @@
 
     @pl.loop(0, n_tp - 1)
     def _(i):
-        pl.semaphore_signal(barrier, inc=1, device_id=(e, tp_peer(i)), device_id_type=MESH)
+        pl.semaphore_signal(barrier, inc=1, device_id=(ep, tp_peer(i)), device_id_type=MESH)
 
     @pl.loop(0, n_ep - 1 - e)
     def _(i):
-        pl.semaphore_signal(barrier, inc=1, device_id=(n_ep - 1 - i, t), device_id_type=MESH)
+        pl.semaphore_signal(barrier, inc=1, device_id=(at_rank(n_ep - 1 - i), t), device_id_type=MESH)
 
     loads(0).wait()
     loads(1).wait()
@@ -106,16 +113,20 @@
         to = tp_peer(i)
         return pltpu.make_async_remote_copy(
             src_ref=q_send.at[pl.ds(to, 1)], dst_ref=q_recv.at[pl.ds(t, 1)],
-            send_sem=q_ss, recv_sem=q_rs, device_id=(e, to), device_id_type=MESH,
+            send_sem=q_ss, recv_sem=q_rs, device_id=(ep, to), device_id_type=MESH,
         )
 
     @pl.loop(0, n_tp - 1, unroll=True)
     def _(i):
         q_copy(i).start()
 
+    late_one = (e >= late).astype(jnp.int32)
+
     @pl.loop(0, e)
     def _(i):
-        pl.semaphore_signal(ready, inc=1, device_id=(i, t), device_id_type=MESH)
+        pl.semaphore_signal(
+            ready.at[late_one], inc=1, device_id=(at_rank(i), t), device_id_type=MESH
+        )
 
     own = iota((rows, 1), 0) == t
     for i in (4, 5, 6, 7):
@@ -147,6 +158,7 @@
         return jnp.sum(jnp.where(eye_rows, row, zero), axis=1, keepdims=True)
 
     chosen = rg[...].reshape(1, -1) * (n_ep // GROUPS) + re[...]
+    chosen = rank_of(chosen)
     slot_row = iota((picks, rows), 0)
     named = jnp.logical_or(
         chosen[0:1, :] == slot_row // SLOTS, chosen[1:2, :] == slot_row // SLOTS
@@ -204,7 +216,7 @@
     def att_copy(i):
         return pltpu.make_async_remote_copy(
             src_ref=att_all.at[t], dst_ref=att_all.at[t],
-            send_sem=a_ss, recv_sem=a_rs, device_id=(e, tp_peer(i)), device_id_type=MESH,
+            send_sem=a_ss, recv_sem=a_rs, device_id=(ep, tp_peer(i)), device_id_type=MESH,
         )
 
     @pl.loop(0, n_tp - 1, unroll=True)
@@ -224,15 +236,11 @@
 
     d_send[...] = dot(place, mixed).astype(BF)
 
-    @pl.when(e < n_ep - 1)
-    def _():
-        pl.semaphore_wait(ready, n_ep - 1 - e)
-
     def pick_copy(to, src, dst, ss, rs):
         return pltpu.make_async_remote_copy(
             src_ref=src.at[pl.ds(pl.multiple_of(to * SLOTS, SLOTS), SLOTS)],
             dst_ref=dst.at[pl.ds(pl.multiple_of(e * SLOTS, SLOTS), SLOTS)],
-            send_sem=ss, recv_sem=rs, device_id=(to, t), device_id_type=MESH,
+            send_sem=ss, recv_sem=rs, device_id=(at_rank(to), t), device_id_type=MESH,
         )
 
     def slots_wait(ref, sem, count):
@@ -241,27 +249,45 @@
 
     batch = sum((e >= first).astype(jnp.int32) for first in bounds[1:-1])
 
-    @pl.loop(0, n_ep - 1, unroll=True)
-    def _(i):
-        pick_copy(ep_peer(i), d_send, d_recv, d_ss, d_rs.at[batch]).start()
+    def send_picks(first, last):
+        @pl.loop(first, last, unroll=True)
+        def _(i):
+            to = i + (i >= e).astype(jnp.int32)
+            pick_copy(to, d_send, d_recv, d_ss, d_rs.at[batch]).start()
+
+    @pl.when(e < late - 1)
+    def _():
+        pl.semaphore_wait(ready.at[0], late - 1 - e)
+
+    send_picks(0, late - 1)
+
+    @pl.when(e < n_ep - 1)
+    def _():
+        pl.semaphore_wait(ready.at[1], jnp.minimum(n_ep - late, n_ep - 1 - e))
+
+    send_picks(late - 1, n_ep - 1)
 
     own_slots = iota((picks, 1), 0) // SLOTS == e
     far_first = sorted(range(1, n_y), key=lambda d: -min(d, n_y - d))
     partner = 2 * y + 1 - c
 
     def column_copy(buf, d, sems):
-        to = 2 * lax.rem(y + d, n_y) + c
+        to = 2 * lax.rem(y + d, n_y) + 1 - c
         return pltpu.make_async_remote_copy(
-            src_ref=buf.at[t], dst_ref=buf.at[t],
-            send_sem=sems.at[0, d], recv_sem=sems.at[1, d], device_id=(e, to), device_id_type=MESH,
+            src_ref=buf.at[t], dst_ref=buf.at[t], send_sem=sems[0].at[0],
+            recv_sem=sems[1].at[d - 1], device_id=(ep, to), device_id_type=MESH,
         )
 
     def pass_on(buf, d, sems):
-        slot = 2 * lax.rem(y + n_y - d, n_y) + c
+        slot = 2 * lax.rem(y + n_y - d, n_y) + (c if d == 0 else 1 - c)
         return pltpu.make_async_remote_copy(
-            src_ref=buf.at[slot], dst_ref=buf.at[slot],
-            send_sem=sems.at[2, d], recv_sem=sems.at[3, d], device_id=(e, partner), device_id_type=MESH,
-        )
+            src_ref=buf.at[slot], dst_ref=buf.at[slot], send_sem=sems[0].at[1],
+            recv_sem=sems[0].at[2], device_id=(ep, partner), device_id_type=MESH,
+        )
+
+    def wait_parts(buf, count, sem):
+        part = buf.at[pl.ds(0, count)]
+        pltpu.make_async_copy(part, part, sem).wait()
 
     def gather_start(buf, sems):
         for d in far_first:
@@ -274,14 +300,11 @@
             pass_on(buf, d, sems).start()
 
     def gather_finish(buf, sems):
-        for d in range(n_y):
-            pass_on(buf, d, sems).wait_recv()
+        wait_parts(buf, n_y, sems[0].at[2])
 
     def gather_end(buf, sems):
-        for d in range(n_y):
-            if d:
-                column_copy(buf, d, sems).wait_send()
-            pass_on(buf, d, sems).wait_send()
+        wait_parts(buf, n_y - 1, sems[0].at[0])
+        wait_parts(buf, n_y, sems[0].at[1])
 
     def arrive(k):
         count = bounds[k + 1] - bounds[k]
@@ -302,9 +325,6 @@
 
     def expand(k):
         gather_finish(x_all[k], x_sems[k])
-        if k == 0:
-            for i in (2, 15, 16, 17):
-                loads(i).wait()
         buf = x_all[k]
         total = jnp.zeros(buf.shape[1:], F32)
         for j in range(n_tp):
@@ -330,26 +350,47 @@
         hidden = jnp.concatenate([h_all[k][j] for j in range(n_tp)], axis=1)
         r_send[slots, :] = dot(hidden, wd[0]).astype(BF)
 
-        @pl.loop(0, n_ep - 1, unroll=True)
-        def _(i):
-            to = ep_peer(i)
-
-            @pl.when(jnp.logical_and(to >= bounds[k], to < bounds[k + 1]))
+        @pl.loop(bounds[k], bounds[k + 1], unroll=True)
+        def _(to):
+            @pl.when(to != e)
             def _():
                 pick_copy(to, r_send, r_recv, r_ss, r_rs).start()
 
     n_batches = len(bounds) - 1
-    arrive(0)
-    gather_pass(x_all[0], x_sems[0])
-    expand(0)
-    for k in range(1, n_batches):
-        arrive(k)
-        gather_pass(h_all[k - 1], h_sems[k - 1])
-        gather_pass(x_all[k], x_sems[k])
-        contract(k - 1)
-        expand(k)
-    gather_pass(h_all[n_batches - 1], h_sems[n_batches - 1])
-    contract(n_batches - 1)
+
+    def work(order):
+        passed = set()
+
+        def once(kind, k):
+            if (kind, k) not in passed:
+                passed.add((kind, k))
+                if kind == "x":
+                    gather_pass(x_all[k], x_sems[k])
+                else:
+                    gather_pass(h_all[k], h_sems[k])
+
+        for step in order.split():
+            kind, k = step[0], int(step[1])
+            if kind == "a":
+                arrive(k)
+            elif kind == "p":
+                once("x", k)
+            elif kind == "q":
+                once("h", k)
+            elif kind == "x":
+                once("x", k)
+                expand(k)
+            else:
+                once("h", k)
+                contract(k)
+
+    for i in (2, 15, 16, 17):
+        loads(i).wait()
+    turn = jnp.where(e == zero_rank, 0, e)
+    for low, high, order in orders:
+        @pl.when(jnp.logical_and(turn >= low, turn < high))
+        def _(order=order):
+            work(order)
 
     slots_wait(r_recv, r_rs, n_ep - 1)
     back = jnp.where(own_slots, r_send[...].astype(F32), r_recv[...].astype(F32)).astype(BF)
@@ -368,7 +409,16 @@
 
 
 def batch_bounds(n_ep):
-    return (0, n_ep // 3, n_ep)
+    return (0, n_ep // 3 - 1, n_ep * 2 // 3, n_ep)
+
+
+def plan_orders(n_ep):
+    early, late = n_ep // 3 - 1, n_ep * 2 // 3
+    return (
+        (0, early, "a0 x0 a1 a2 q0 p1 x1 p2 x2 h0 h1 h2"),
+        (early, late, "a0 x0 a1 q0 p1 a2 h0 x1 p2 x2 h1 h2"),
+        (late, n_ep, "a0 a1 a2 x0 x1 x2 h0 h1 h2"),
+    )
 
 
 def on_device(*args):
@@ -399,14 +449,15 @@
     ]
     scratch += [pltpu.VMEM((n_tp, size, width), BF) for size in sizes + sizes]
     scratch += [dma((18,)), dma, dma, dma, dma, dma, dma, dma((len(sizes),)), dma, dma]
-    scratch += [pltpu.SemaphoreType.REGULAR]
-    scratch += [dma((4, n_tp // 2)) for _ in sizes + sizes]
+    scratch += [pltpu.SemaphoreType.REGULAR((2,))]
+    for _ in range(2):
+        scratch += [dma((3,)) for _ in sizes] + [dma((n_tp // 2 - 1,)) for _ in sizes]
     args = [
         a if i == 12 else pltpu.with_memory_space_constraint(a, pltpu.HBM)
         for i, a in enumerate(args)
     ]
     return pl.pallas_call(
-        functools.partial(layer_kernel, n_ep, n_tp, bounds),
+        functools.partial(layer_kernel, n_ep, n_tp, bounds, plan_orders(n_ep)),
         out_shape=jax.ShapeDtypeStruct((rows, width), F32),
         in_specs=specs,
         out_specs=pl.BlockSpec(memory_space=pltpu.VMEM),

time: 54.9 us -> 55.7 us (1.015)
  Pallas kernels: 53.5 us -> 54.3 us
    pallas_call x1, Pallas kernels: 53.5 us -> 54.3 us  [on_device(): pl.pallas_call(functools.partial(layer_kernel, n_ep, n_tp, bounds, plan_o...]
where the time goes in v3:
time: 55.7 us; the launch traced here: 55.6 us
  Pallas kernels  54.3 us (97%)
  between operations  0.66 us (1%)
  other arithmetic  0.6 us (1%)
    pallas_call x1, Pallas kernels, on_device(): pl.pallas_call(functools.partial(layer_kernel, n_ep, n_tp, bounds, plan_o...  54.3 us

profile of v3, /device:TPU:1, one launch (start us, length us, event | category | flops | bytes accessed | tf_op | source)
XLA Modules:
  0.0 55.6 jit_solution(13987965785196309208)
XLA Ops:
  0.7 54.3 %layer.1 = f32[16,128]{1,0:T(8,128)S(1)} custom-call(bf16[16,2048]{1,0:T(8,128)(2,1)} %refs_0_.1, bf16[2048]{0:T(1024)(128)(2,1)} %refs_1_.1, bf16[2048]{0:T(1024)(128)(2,1)} %refs_2_.1, bf16[2048,128]{1,0:T(8,128)(2,1)} %refs_3_.1, bf16[2048,256]{1,0:T(8,128)(2,1)} %refs_4_.1, bf16[2048,256]{1,0:T(8,128)(2,1)} %refs_5_.1, bf16[32,2048]{1,0:T(8,128)(2,1)} %bitcast.3, ...), custom_call_target="tpu_custom_call" | custom-call | tf_op jit(solution)/shard_map/layer/pallas_call | solution.py:459
  55.0 0.6 %convert_element_type.3 = bf16[16,128]{1,0:T(8,128)(2,1)} convert(f32[16,128]{1,0:T(8,128)S(1)} %layer.1) | non-fusion elementwise | flops 2048 | bytes 12288 | tf_op jit(solution)/shard_map/convert_element_type | solution.py:469

commit v4 on v3

--- a/solution.py
+++ b/solution.py
@@ -51,7 +51,7 @@
         del scratch[:number]
         return taken
 
-    q_send, q_recv, att_all, att_rows, d_send, d_recv, r_send, r_recv, len_ref = take(9)
+    q_send, q_recv, att_all, att_rows, d_send, d_recv, r_send, r_recv, decay, len_ref = take(10)
     x_all, h_all = take(count), take(count)
     in_sem, len_sem, q_ss, q_rs, a_ss, a_rs, d_ss, d_rs, r_ss, r_rs, ready = take(11)
     x_sems = list(zip(take(count), take(count)))
@@ -101,9 +101,15 @@
     scale = lax.rsqrt(jnp.mean(stream * stream, axis=-1, keepdims=True) + EPSILON)
     normed = (stream * scale * again[...].reshape(1, -1).astype(F32)).astype(BF)
     loads(3).wait()
-    for i in (4, 5, 6, 7, 11):
+    for i in (4, 5, 6, 7):
         loads(i).start()
     load_len.start()
+    for row in range(HEADS):
+        pltpu.make_async_copy(
+            sources[11].at[0, pl.ds(2 * (row % n_tp) + row // n_tp, 1)],
+            lc.at[0, pl.ds(row, 1)],
+            in_sem.at[11],
+        ).start()
     for i in (12, 13, 14, 9, 10, 8, 2, 15, 16, 17):
         loads(i).start()
     q_send[...] = dot(normed, wq[...]).astype(BF).astype(F32)
@@ -137,11 +143,11 @@
 
     key_new = own_row(dot(normed, wk[...])).astype(BF).astype(F32)
     value_new = own_row(dot(normed, wv[...])).astype(BF).astype(F32)
-    eye = iota((HEADS, HEADS), 0) == iota((HEADS, HEADS), 1)
-    bias = jnp.sum(jnp.where(eye, fb[...].reshape(1, -1), 0.0), axis=1, keepdims=True)
-    gate_all = dot_t(wf[...], normed)
-    own_lane = iota((1, rows), 1) == t
-    gate_in = jnp.sum(jnp.where(own_lane, gate_all, 0.0), axis=1, keepdims=True) + bias
+    head = 2 * (iota((HEADS, 1), 0) % n_tp) + iota((HEADS, 1), 0) // n_tp
+    head_lane = head == iota((HEADS, HEADS), 1)
+    bias = jnp.sum(jnp.where(head_lane, fb[...].reshape(1, -1), 0.0), axis=1, keepdims=True)
+    gate_all = dot_t(normed, wf[...])
+    gate_in = jnp.sum(jnp.where(head_lane, own_row(gate_all), 0.0), axis=1, keepdims=True) + bias
     log_gate = jnp.minimum(gate_in, 0.0) - jnp.log1p(jnp.exp(-jnp.abs(gate_in)))
     loads(11).wait()
     load_len.wait()
@@ -149,6 +155,7 @@
     logcum = lc[0]
     position = iota((1, logcum.shape[1]), 1)
     latest = jnp.sum(jnp.where(position == length - 1, logcum, 0.0), axis=1, keepdims=True)
+    decay[...] = jnp.where(position < length, (latest + log_gate) - logcum, MASKED_SCORE)
 
     for i in (12, 13, 14):
         loads(i).wait()
@@ -178,26 +185,21 @@
     combine = exact_parts(jnp.where(here, named_t * weight_t, 0.0))
 
     pltpu.make_async_copy(q_recv.at[pl.ds(0, n_tp - 1)], q_recv.at[pl.ds(0, n_tp - 1)], q_rs).wait()
-    q16 = jnp.where(iota((n_tp, 1), 0) == t, q_send[...], q_recv[...])
-    twice = (iota((HEADS, n_tp), 0) // 2 == iota((HEADS, n_tp), 1)).astype(F32).astype(BF)
-    q32 = dot(twice, q16.astype(BF))
-    turned = pltpu.roll(q32, HEAD, 1)
-    odd = iota((HEADS, 2 * HEAD), 0) % 2 == 1
-    low = iota((HEADS, 2 * HEAD), 1) < HEAD
-    q_both = jnp.where(odd == low, turned, q32)
+    q16 = jnp.where(iota((n_tp, 1), 0) == t, q_send[...], q_recv[...]) * (HEAD ** (-0.5))
+    turned = pltpu.roll(q16, HEAD, 1)
+    low = iota((n_tp, 2 * HEAD), 1) < HEAD
+    q_both = jnp.concatenate(
+        [jnp.where(low, q16, turned), jnp.where(low, turned, q16)], axis=0
+    )
     q_wide = jnp.concatenate([q_both] * (KV_HEADS // 2), axis=1)
     kv_width = KV_HEADS * HEAD
-    mine = iota((HEADS, kv_width), 1) // HEAD == iota((HEADS, kv_width), 0) // (HEADS // KV_HEADS)
+    mine = iota((HEADS, kv_width), 1) // HEAD == head // (HEADS // KV_HEADS)
     q_wide = jnp.where(mine, q_wide, 0.0)
-    score_scale = HEAD ** (-0.5)
-    own_score = jnp.sum(q_wide * key_new, axis=1, keepdims=True) * score_scale
+    own_score = jnp.sum(q_wide * key_new, axis=1, keepdims=True)
     loads(9).wait()
-    scores = dot_t(q_wide.astype(BF), ck[0]) * score_scale
-    scores = scores + latest + log_gate - logcum
-    usable = position < length
-    scores = jnp.where(usable, scores, MASKED_SCORE)
+    scores = dot_t(q_wide.astype(BF), ck[0]) + decay[...]
     peak = jnp.maximum(jnp.max(scores, axis=1, keepdims=True), own_score)
-    weights = jnp.where(usable, jnp.exp(scores - peak), 0.0)
+    weights = jnp.exp(scores - peak)
     own_weight = jnp.exp(own_score - peak)
     denominator = jnp.sum(weights, axis=1, keepdims=True) + own_weight
     loads(10).wait()
@@ -207,11 +209,8 @@
     folded = summed[:, : 2 * HEAD]
     for k in range(1, KV_HEADS // 2):
         folded = folded + summed[:, k * 2 * HEAD : (k + 1) * 2 * HEAD]
-    folded = ((folded + pltpu.roll(folded, HEAD, 1)) / denominator).astype(BF)
-    pair = iota((n_tp, HEADS), 1) - 2 * iota((n_tp, HEADS), 0)
-    even_rows = dot((pair == 0).astype(F32).astype(BF), folded)
-    odd_rows = dot((pair == 1).astype(F32).astype(BF), folded)
-    att_all[t] = jnp.where(iota((n_tp, 2 * HEAD), 1) < HEAD, even_rows, odd_rows).astype(BF)
+    folded = (folded + pltpu.roll(folded, HEAD, 1)) / denominator
+    att_all[t] = jnp.where(low, folded[:n_tp], folded[n_tp:]).astype(BF)
 
     def att_copy(i):
         return pltpu.make_async_remote_copy(
@@ -386,9 +385,8 @@
 
     for i in (2, 15, 16, 17):
         loads(i).wait()
-    turn = jnp.where(e == zero_rank, 0, e)
     for low, high, order in orders:
-        @pl.when(jnp.logical_and(turn >= low, turn < high))
+        @pl.when(jnp.logical_and(e >= low, e < high))
         def _(order=order):
             work(order)
 
@@ -409,14 +407,15 @@
 
 
 def batch_bounds(n_ep):
-    return (0, n_ep // 3 - 1, n_ep * 2 // 3, n_ep)
+    return (0, n_ep // 3, n_ep * 2 // 3, n_ep)
 
 
 def plan_orders(n_ep):
-    early, late = n_ep // 3 - 1, n_ep * 2 // 3
+    early, middle, late = n_ep // 3, n_ep // 2, n_ep * 2 // 3
     return (
         (0, early, "a0 x0 a1 a2 q0 p1 x1 p2 x2 h0 h1 h2"),
-        (early, late, "a0 x0 a1 q0 p1 a2 h0 x1 p2 x2 h1 h2"),
+        (early, middle, "a0 x0 a1 a2 q0 p1 h0 x1 p2 x2 h1 h2"),
+        (middle, late, "a0 a1 x0 a2 x1 h0 x2 h1 h2"),
         (late, n_ep, "a0 a1 a2 x0 x1 x2 h0 h1 h2"),
     )
 
@@ -445,6 +444,7 @@
         pltpu.VMEM((picks, width), BF),
         pltpu.VMEM((picks, width), BF),
         pltpu.VMEM((picks, width), BF),
+        pltpu.VMEM(args[11].shape[1:], F32),
         pltpu.SMEM((1,), jnp.int32),
     ]
     scratch += [pltpu.VMEM((n_tp, size, width), BF) for size in sizes + sizes]

time: 55.7 us -> 52 us (0.934)
  Pallas kernels: 54.3 us -> 50.6 us
    pallas_call x1, Pallas kernels: 54.3 us -> 50.6 us  [on_device(): pl.pallas_call(functools.partial(layer_kernel, n_ep, n_tp, bounds, plan_o...]
where the time goes in v4:
time: 52 us; the launch traced here: 51.8 us
  Pallas kernels  50.6 us (97%)
  between operations  0.66 us (1%)
  other arithmetic  0.6 us (1%)
    pallas_call x1, Pallas kernels, on_device(): pl.pallas_call(functools.partial(layer_kernel, n_ep, n_tp, bounds, plan_o...  50.6 us

profile of v4, /device:TPU:1, one launch (start us, length us, event | category | flops | bytes accessed | tf_op | source)
XLA Modules:
  0.0 51.8 jit_solution(4565001126090648477)
XLA Ops:
  0.7 50.6 %layer.1 = f32[16,128]{1,0:T(8,128)S(1)} custom-call(bf16[16,2048]{1,0:T(8,128)(2,1)} %refs_0_.1, bf16[2048]{0:T(1024)(128)(2,1)} %refs_1_.1, bf16[2048]{0:T(1024)(128)(2,1)} %refs_2_.1, bf16[2048,128]{1,0:T(8,128)(2,1)} %refs_3_.1, bf16[2048,256]{1,0:T(8,128)(2,1)} %refs_4_.1, bf16[2048,256]{1,0:T(8,128)(2,1)} %refs_5_.1, bf16[32,2048]{1,0:T(8,128)(2,1)} %bitcast.3, ...), custom_call_target="tpu_custom_call" | custom-call | tf_op jit(solution)/shard_map/layer/pallas_call | solution.py:459
  51.2 0.6 %convert_element_type.3 = bf16[16,128]{1,0:T(8,128)(2,1)} convert(f32[16,128]{1,0:T(8,128)S(1)} %layer.1) | non-fusion elementwise | flops 2048 | bytes 12288 | tf_op jit(solution)/shard_map/convert_element_type | solution.py:469

commit v5 on v4

--- a/solution.py
+++ b/solution.py
@@ -51,11 +51,10 @@
         del scratch[:number]
         return taken
 
-    q_send, q_recv, att_all, att_rows, d_send, d_recv, r_send, r_recv, decay, len_ref = take(10)
+    q_send, q_recv, att_all, att_rows, d_send, d_recv, r_send, r_recv, decay, keys_t, len_ref = take(11)
     x_all, h_all = take(count), take(count)
     in_sem, len_sem, q_ss, q_rs, a_ss, a_rs, d_ss, d_rs, r_ss, r_rs, ready = take(11)
-    x_sems = list(zip(take(count), take(count)))
-    h_sems = list(zip(take(count), take(count)))
+    x_sems, h_sems = take(count), take(count)
     ep = lax.axis_index("ep")
     zero_rank = n_ep // 3 - 1
 
@@ -184,6 +183,9 @@
     weight_t = jnp.where(first, column(rw[0:1, :], 0.0), column(rw[1:2, :], 0.0))
     combine = exact_parts(jnp.where(here, named_t * weight_t, 0.0))
 
+    loads(9).wait()
+    keys_t[...] = ck[0].T
+
     pltpu.make_async_copy(q_recv.at[pl.ds(0, n_tp - 1)], q_recv.at[pl.ds(0, n_tp - 1)], q_rs).wait()
     q16 = jnp.where(iota((n_tp, 1), 0) == t, q_send[...], q_recv[...]) * (HEAD ** (-0.5))
     turned = pltpu.roll(q16, HEAD, 1)
@@ -196,8 +198,7 @@
     mine = iota((HEADS, kv_width), 1) // HEAD == head // (HEADS // KV_HEADS)
     q_wide = jnp.where(mine, q_wide, 0.0)
     own_score = jnp.sum(q_wide * key_new, axis=1, keepdims=True)
-    loads(9).wait()
-    scores = dot_t(q_wide.astype(BF), ck[0]) + decay[...]
+    scores = dot(q_wide.astype(BF), keys_t[...]) + decay[...]
     peak = jnp.maximum(jnp.max(scores, axis=1, keepdims=True), own_score)
     weights = jnp.exp(scores - peak)
     own_weight = jnp.exp(own_score - peak)
@@ -273,15 +274,15 @@
     def column_copy(buf, d, sems):
         to = 2 * lax.rem(y + d, n_y) + 1 - c
         return pltpu.make_async_remote_copy(
-            src_ref=buf.at[t], dst_ref=buf.at[t], send_sem=sems[0].at[0],
-            recv_sem=sems[1].at[d - 1], device_id=(ep, to), device_id_type=MESH,
+            src_ref=buf.at[t], dst_ref=buf.at[t], send_sem=sems.at[0],
+            recv_sem=sems.at[1 + min(d, n_y - d)], device_id=(ep, to), device_id_type=MESH,
         )
 
     def pass_on(buf, d, sems):
         slot = 2 * lax.rem(y + n_y - d, n_y) + (c if d == 0 else 1 - c)
         return pltpu.make_async_remote_copy(
-            src_ref=buf.at[slot], dst_ref=buf.at[slot], send_sem=sems[0].at[1],
-            recv_sem=sems[0].at[2], device_id=(ep, partner), device_id_type=MESH,
+            src_ref=buf.at[slot], dst_ref=buf.at[slot], send_sem=sems.at[0],
+            recv_sem=sems.at[1], device_id=(ep, partner), device_id_type=MESH,
         )
 
     def wait_parts(buf, count, sem):
@@ -294,16 +295,17 @@
         pass_on(buf, 0, sems).start()
 
     def gather_pass(buf, sems):
-        for d in far_first[::-1]:
-            column_copy(buf, d, sems).wait_recv()
-            pass_on(buf, d, sems).start()
+        for d in range(1, n_y // 2 + 1):
+            both = sorted({d, n_y - d})
+            wait_parts(buf, len(both), sems.at[1 + d])
+            for side in both:
+                pass_on(buf, side, sems).start()
 
     def gather_finish(buf, sems):
-        wait_parts(buf, n_y, sems[0].at[2])
+        wait_parts(buf, n_y, sems.at[1])
 
     def gather_end(buf, sems):
-        wait_parts(buf, n_y - 1, sems[0].at[0])
-        wait_parts(buf, n_y, sems[0].at[1])
+        wait_parts(buf, 2 * n_y - 1, sems.at[0])
 
     def arrive(k):
         count = bounds[k + 1] - bounds[k]
@@ -407,7 +409,7 @@
 
 
 def batch_bounds(n_ep):
-    return (0, n_ep // 3, n_ep * 2 // 3, n_ep)
+    return (0, n_ep // 3, n_ep // 2, n_ep)
 
 
 def plan_orders(n_ep):
@@ -445,13 +447,13 @@
         pltpu.VMEM((picks, width), BF),
         pltpu.VMEM((picks, width), BF),
         pltpu.VMEM(args[11].shape[1:], F32),
+        pltpu.VMEM(args[9].shape[:0:-1], BF),
         pltpu.SMEM((1,), jnp.int32),
     ]
     scratch += [pltpu.VMEM((n_tp, size, width), BF) for size in sizes + sizes]
     scratch += [dma((18,)), dma, dma, dma, dma, dma, dma, dma((len(sizes),)), dma, dma]
     scratch += [pltpu.SemaphoreType.REGULAR((2,))]
-    for _ in range(2):
-        scratch += [dma((3,)) for _ in sizes] + [dma((n_tp // 2 - 1,)) for _ in sizes]
+    scratch += [dma((2 + n_tp // 4,)) for _ in sizes + sizes]
     args = [
         a if i == 12 else pltpu.with_memory_space_constraint(a, pltpu.HBM)
         for i, a in enumerate(args)

time: 52 us -> 50.7 us (0.975)
  Pallas kernels: 50.6 us -> 49.3 us
    pallas_call x1, Pallas kernels: 50.6 us -> 49.3 us  [on_device(): pl.pallas_call(functools.partial(layer_kernel, n_ep, n_tp, bounds, plan_o...]
where the time goes in v5:
time: 50.7 us; the launch traced here: 50.5 us
  Pallas kernels  49.3 us (97%)
  between operations  0.66 us (1%)
  other arithmetic  0.6 us (1%)
    pallas_call x1, Pallas kernels, on_device(): pl.pallas_call(functools.partial(layer_kernel, n_ep, n_tp, bounds, plan_o...  49.3 us

profile of v5, /device:TPU:1, one launch (start us, length us, event | category | flops | bytes accessed | tf_op | source)
XLA Modules:
  0.0 50.5 jit_solution(14147096825179505871)
XLA Ops:
  0.7 49.3 %layer.1 = f32[16,128]{1,0:T(8,128)S(1)} custom-call(bf16[16,2048]{1,0:T(8,128)(2,1)} %refs_0_.1, bf16[2048]{0:T(1024)(128)(2,1)} %refs_1_.1, bf16[2048]{0:T(1024)(128)(2,1)} %refs_2_.1, bf16[2048,128]{1,0:T(8,128)(2,1)} %refs_3_.1, bf16[2048,256]{1,0:T(8,128)(2,1)} %refs_4_.1, bf16[2048,256]{1,0:T(8,128)(2,1)} %refs_5_.1, bf16[32,2048]{1,0:T(8,128)(2,1)} %bitcast.3, ...), custom_call_target="tpu_custom_call" | custom-call | tf_op jit(solution)/shard_map/layer/pallas_call | solution.py:461
  49.9 0.6 %convert_element_type.3 = bf16[16,128]{1,0:T(8,128)(2,1)} convert(f32[16,128]{1,0:T(8,128)S(1)} %layer.1) | non-fusion elementwise | flops 2048 | bytes 12288 | tf_op jit(solution)/shard_map/convert_element_type | solution.py:471

commit v6 on v5

--- a/solution.py
+++ b/solution.py
@@ -415,7 +415,7 @@
 def plan_orders(n_ep):
     early, middle, late = n_ep // 3, n_ep // 2, n_ep * 2 // 3
     return (
-        (0, early, "a0 x0 a1 a2 q0 p1 x1 p2 x2 h0 h1 h2"),
+        (0, early, "a0 x0 a1 a2 q0 p1 p2 h0 x1 x2 q1 q2 h1 h2"),
         (early, middle, "a0 x0 a1 a2 q0 p1 h0 x1 p2 x2 h1 h2"),
         (middle, late, "a0 a1 x0 a2 x1 h0 x2 h1 h2"),
         (late, n_ep, "a0 a1 a2 x0 x1 x2 h0 h1 h2"),

time: 50.7 us -> 50.2 us (level)
  no operation moved by 1% of the time
where the time goes in v6:
time: 50.2 us; the launch traced here: 50 us
  Pallas kernels  48.8 us (97%)
  between operations  0.66 us (1%)
  other arithmetic  0.6 us (1%)
    pallas_call x1, Pallas kernels, on_device(): pl.pallas_call(functools.partial(layer_kernel, n_ep, n_tp, bounds, plan_o...  48.8 us

profile of v6, /device:TPU:1, one launch (start us, length us, event | category | flops | bytes accessed | tf_op | source)
XLA Modules:
  0.0 50.0 jit_solution(15395814693786117289)
XLA Ops:
  0.7 48.8 %layer.1 = f32[16,128]{1,0:T(8,128)S(1)} custom-call(bf16[16,2048]{1,0:T(8,128)(2,1)} %refs_0_.1, bf16[2048]{0:T(1024)(128)(2,1)} %refs_1_.1, bf16[2048]{0:T(1024)(128)(2,1)} %refs_2_.1, bf16[2048,128]{1,0:T(8,128)(2,1)} %refs_3_.1, bf16[2048,256]{1,0:T(8,128)(2,1)} %refs_4_.1, bf16[2048,256]{1,0:T(8,128)(2,1)} %refs_5_.1, bf16[32,2048]{1,0:T(8,128)(2,1)} %bitcast.3, ...), custom_call_target="tpu_custom_call" | custom-call | tf_op jit(solution)/shard_map/layer/pallas_call | solution.py:461
  49.4 0.6 %convert_element_type.3 = bf16[16,128]{1,0:T(8,128)(2,1)} convert(f32[16,128]{1,0:T(8,128)S(1)} %layer.1) | non-fusion elementwise | flops 2048 | bytes 12288 | tf_op jit(solution)/shard_map/convert_element_type | solution.py:471
